TPU v7x, 32 devices: a whole 2x2x4 slice. The times are simulated.
32 devices in a mesh: gr: 2 (over core), fs: 8 (over z, y), tp: 2 (over x).
Axes of the slice: x: 2, y: 2, z: 4, core: 2. Of those that a mesh axis runs over, the one named last changes fastest.
Arguments:
- prompt: bfloat16 [5120, 2048], P(('gr', 'fs'), 'tp'), may hold values from -6 to 6
- norm_gain: float32 [2048], P(('gr', 'fs')), may hold values from 0.1 to 1.9
- gate_weight: float32 [32, 2048, 2048], P(None, ('gr', 'fs'), 'tp'), may hold values from -0.125 to 0.125
- up_weight: float32 [32, 2048, 2048], P(None, ('gr', 'fs'), 'tp'), may hold values from -0.125 to 0.125
- down_weight: float32 [32, 2048, 2048], P(None, ('gr', 'fs'), 'tp'), may hold values from -0.125 to 0.125
- routes: int32 [5120, 2], P(('gr', 'fs')), may hold values from 0 to 31, as said below
- route_weight: float32 [5120, 2], P(('gr', 'fs')), may hold values from 0.2 to 1
Outputs:
- gate_new: bfloat16 [32, 2048, 2048], P('fs', None, 'tp')
- up_new: bfloat16 [32, 2048, 2048], P('fs', None, 'tp')
- down_new: bfloat16 [32, 2048, 2048], P('fs', 'tp')
- mixed: bfloat16 [5120, 2048], P(('gr', 'fs'), 'tp')
Inputs may be any that keep to these rules, and one draw needn't show every extreme that they name: `routes`: each row names two different experts of the same group; expert e belongs to group e // 8. Among the 320 rows of one index of gr and fs no expert is named more than 30 times, and in every draw every expert of one group is named exactly 30 times by the rows of every index.
All inputs are finite; a program needn't handle non-finite values.
Results may differ from a plain program's by a relative error of at most 0.015.
Values may be sent and summed in bfloat16 or wider, within the bound.
A program may use at most 256 MiB of HBM per device.

v0:
```python
import functools

import jax
import jax.numpy as jnp
from jax import lax
from jax.experimental import pallas as pl
from jax.experimental.pallas import tpu as pltpu
from jax.sharding import PartitionSpec as P

CAP = 30
SLOT = -(-CAP // 16) * 16
MESH = pl.DeviceIdType.MESH


def remote(src, dst, send, recv, device):
    copy = pltpu.make_async_remote_copy(
        src_ref=src, dst_ref=dst, send_sem=send, recv_sem=recv, device_id=device, device_id_type=MESH
    )
    copy.start()


def settle(ref, sem):
    pltpu.make_async_copy(ref, ref, sem).wait()


def loop(low, high, step):
    lax.fori_loop(low, high, lambda index, carry: (step(index), carry)[1], 0)


def span(index, size):
    return pl.ds(pl.multiple_of(index * size, size), size)


def greet(barrier, device):
    pl.semaphore_signal(barrier, inc=1, device_id=device, device_id_type=MESH)


def spread_kernel(
    sizes, tok, gate, up, down, arr, gate_out, up_out, down_out,
    own_tok, own, tok_send, tok_recv, share_send, share_recv,
    w_send, w_recv, twin_send, twin_recv, own_sem,
):
    n_gr, n_fs, n_tp = sizes
    gr, fs, tp = lax.axis_index("gr"), lax.axis_index("fs"), lax.axis_index("tp")
    per, blk, wide = gate_out.shape[0], gate.shape[1], gate.shape[2]
    per_tp = n_gr * n_fs // n_tp
    row = gr * n_fs + fs
    owner = row // per_tp
    home = tp * per_tp // n_fs
    ring = n_fs * n_tp

    barrier = pltpu.get_barrier_semaphore()

    def greet_plane(k):
        other = (fs * n_tp + tp + k) % ring
        greet(barrier, (gr, other // n_tp, other % n_tp))

    loop(1, ring, greet_plane)
    loop(1, n_gr, lambda k: greet(barrier, ((gr + k) % n_gr, fs, tp)))
    pl.semaphore_wait(barrier, ring + n_gr - 2)

    def tok_place(source, t):
        return arr.at[:, source, :, span(t, wide)]

    def rows_of(out, index):
        return out.at[:, span(index, blk), :]

    def down_place(index):
        return down_out.at[:, span(index, blk), span(tp, wide)]

    def mine(ref, f):
        return ref.at[pl.ds(f * per, per)]

    loads = [pltpu.make_async_copy(tok.at[fs], own_tok, own_sem.at[3])]
    for w, ref in enumerate((gate, up, down)):
        loads.append(pltpu.make_async_copy(mine(ref, fs), own.at[w], own_sem.at[w]))
    for load in loads:
        load.start()

    def far(k):
        return (fs + (k + n_fs // 2 - 1) % (n_fs - 1) + 1) % n_fs

    def send_tok(k):
        f = far(k)
        remote(tok.at[f], tok_place(fs, tp), tok_send, tok_recv.at[fs], (gr, f, tp))

    loop(0, n_fs - 1, send_tok)

    def send_down(k):
        f = far(k)
        remote(mine(down, f), down_place(row - owner * per_tp), w_send.at[2], w_recv.at[2, fs], (gr, f, owner))

    loop(0, n_fs - 1, send_down)
    for w, (ref, out) in enumerate(((gate, gate_out), (up, up_out))):

        def send_w(k, w=w, ref=ref, out=out):
            f = far(k)
            remote(mine(ref, f), rows_of(out, row), w_send.at[w], w_recv.at[w, fs], (gr, f, tp))

        loop(0, n_fs - 1, send_w)

    for load in loads:
        load.wait()
    pltpu.make_async_copy(own_tok, tok_place(fs, tp), tok_recv.at[fs]).start()
    pltpu.make_async_copy(own.at[0], rows_of(gate_out, row), w_recv.at[0, fs]).start()
    pltpu.make_async_copy(own.at[1], rows_of(up_out, row), w_recv.at[1, fs]).start()

    @pl.when(owner == tp)
    def _():
        pltpu.make_async_copy(own.at[2], down_place(row - owner * per_tp), w_recv.at[2, fs]).start()

    @pl.when(owner != tp)
    def _():
        remote(own.at[2], down_place(row - owner * per_tp), w_send.at[2], w_recv.at[2, fs], (gr, fs, owner))

    def share_tok(k):
        source = (fs + n_fs - k) % n_fs
        place = tok_place(source, tp)
        settle(place, tok_recv.at[source])
        for j in range(1, n_tp):
            t = (tp + j) % n_tp
            remote(place, place, share_send.at[t], share_recv.at[tp], (gr, fs, t))

    loop(0, n_fs, share_tok)

    @pl.when(home == gr)
    def _():
        def twin_down(k):
            source = tp * per_tp - gr * n_fs + k
            place = rows_of(down_out, k)
            settle(place, w_recv.at[2, source])
            for j in range(1, n_gr):
                g = (gr + j) % n_gr
                remote(place, place, twin_send.at[2, g], twin_recv.at[2, gr], (g, fs, tp))

        loop(0, per_tp, twin_down)

    for w, out in enumerate((gate_out, up_out)):

        def twin_w(k, w=w, out=out):
            source = (fs + n_fs - k) % n_fs
            place = rows_of(out, gr * n_fs + source)
            settle(place, w_recv.at[w, source])
            for j in range(1, n_gr):
                g = (gr + j) % n_gr
                remote(place, place, twin_send.at[w, g], twin_recv.at[w, gr], (g, fs, tp))

        loop(0, n_fs, twin_w)

    settle(tok.at[pl.ds(0, n_fs - 1)], tok_send)
    for w, ref in enumerate((gate, up)):
        settle(ref.at[pl.ds(0, (n_fs - 1) * per)], w_send.at[w])

    @pl.when(owner == tp)
    def _():
        settle(down.at[pl.ds(0, (n_fs - 1) * per)], w_send.at[2])

    @pl.when(owner != tp)
    def _():
        settle(down, w_send.at[2])

    for j in range(1, n_tp):
        t = (tp + j) % n_tp
        settle(arr.at[:, :, :, span(tp, wide)], share_send.at[t])
        settle(arr.at[:, :, :, span(t, wide)], share_recv.at[t])
    for j in range(1, n_gr):
        g = (gr + j) % n_gr
        for w, out in enumerate((gate_out, up_out)):
            settle(out.at[:, span(gr, n_fs * blk), :], twin_send.at[w, g])
            settle(out.at[:, span(g, n_fs * blk), :], twin_recv.at[w, g])

        @pl.when(home == gr)
        def _():
            settle(down_out, twin_send.at[2, g])

    @pl.when(home != gr)
    def _():
        settle(down_out, twin_recv.at[2, home])


def return_kernel(sizes, part, ret, got, summed, x_send, x_recv, z_send, z_recv):
    n_gr, n_fs, n_tp = sizes
    gr, fs, tp = lax.axis_index("gr"), lax.axis_index("fs"), lax.axis_index("tp")
    per, wide = part.shape[0], ret.shape[3]

    barrier = pltpu.get_barrier_semaphore()
    loop(1, n_fs, lambda k: greet(barrier, (gr, (fs + k) % n_fs, tp)))
    loop(1, n_tp, lambda k: greet(barrier, (gr, fs, (tp + k) % n_tp)))
    pl.semaphore_wait(barrier, n_fs + n_tp - 2)

    def exchange(x):
        for j in range(1, n_tp):
            t = (tp + j) % n_tp
            remote(part.at[x, :, :, span(t, wide)], got.at[tp, x], x_send.at[t], x_recv.at[tp, x], (gr, fs, t))

    loop(0, per, exchange)

    def reduce_one(x):
        for j in range(1, n_tp):
            t = (tp + j) % n_tp
            settle(got.at[t, x], x_recv.at[t, x])

        def add(f):
            total = part[x, f, :, span(tp, wide)].astype(jnp.float32)
            for j in range(1, n_tp):
                total = total + got[(tp + j) % n_tp, x, f].astype(jnp.float32)
            summed[x, f] = total.astype(jnp.bfloat16)

        loop(0, n_fs, add)
        ret[fs, x] = summed[x, fs]

        def send(k):
            f = (fs + (k + n_fs // 2 - 1) % (n_fs - 1) + 1) % n_fs
            remote(summed.at[x, f], ret.at[fs, x], z_send, z_recv.at[fs], (gr, f, tp))

        loop(0, n_fs - 1, send)

    loop(0, per, reduce_one)
    loop(1, n_fs, lambda k: settle(ret.at[(fs + k) % n_fs], z_recv.at[(fs + k) % n_fs]))
    settle(summed.at[:, pl.ds(0, n_fs - 1)], z_send)
    for j in range(1, n_tp):
        t = (tp + j) % n_tp
        settle(part.at[:, :, :, span(t, wide)], x_send.at[t])


def hidden_kernel(rows, gate, up, hidden, gate_out, up_out):
    gate_out[...] = gate[...]
    up_out[...] = up[...]
    gate_pre = jnp.dot(rows[0], gate[0], preferred_element_type=jnp.float32)
    up_pre = jnp.dot(rows[0], up[0], preferred_element_type=jnp.float32)
    hidden[0] = (jax.nn.silu(gate_pre) * up_pre).astype(hidden.dtype)


def down_kernel(rows, down, part, down_out):
    down_out[...] = down[...]
    part[0] = jnp.dot(rows[0], down[0], preferred_element_type=jnp.float32).astype(part.dtype)


def expert_call(kernel, rows, *weights):
    per, count, depth = rows.shape
    wide = weights[0].shape[2]
    tile = min(wide, 512)
    rows_spec = pl.BlockSpec((1, count, depth), lambda x, c: (x, 0, 0))
    weight_spec = pl.BlockSpec((1, depth, tile), lambda x, c: (x, 0, c))
    result_spec = pl.BlockSpec((1, count, tile), lambda x, c: (x, 0, c))
    return pl.pallas_call(
        kernel,
        grid=(per, wide // tile),
        out_shape=(
            jax.ShapeDtypeStruct((per, count, wide), rows.dtype),
            *(jax.ShapeDtypeStruct(weight.shape, weight.dtype) for weight in weights),
        ),
        in_specs=[rows_spec] + [weight_spec] * len(weights),
        out_specs=(result_spec,) + (weight_spec,) * len(weights),
        compiler_params=pltpu.CompilerParams(vmem_limit_bytes=56 * 1024 * 1024),
    )(rows, *weights)


def body(sizes, prompt, norm_gain, gate_weight, up_weight, down_weight, routes, route_weight):
    n_gr, n_fs, n_tp = sizes
    gate_cast = (gate_weight * norm_gain[None, :, None]).astype(jnp.bfloat16)
    up_cast = (up_weight * norm_gain[None, :, None]).astype(jnp.bfloat16)
    down_cast = down_weight.astype(jnp.bfloat16)
    values = prompt.astype(jnp.float32)
    tok_count, wide = prompt.shape
    full_width = wide * n_tp
    squares = jnp.sum(values * values, axis=-1, keepdims=True)
    total_squares = lax.psum(squares, "tp")
    normed = (values * lax.rsqrt(total_squares / full_width + 1e-06)).astype(jnp.bfloat16)
    experts, blk, _ = gate_weight.shape
    per = experts // n_fs
    slots_all = experts * SLOT
    picks_flat = routes.reshape(-1)
    matches = picks_flat[:, None] == jnp.arange(experts, dtype=jnp.int32)[None, :]
    order = jnp.arange(2 * tok_count, dtype=jnp.int32)
    before = (order[None, :] < order[:, None]).astype(jnp.bfloat16)
    earlier = jnp.dot(before, matches.astype(jnp.bfloat16), preferred_element_type=jnp.float32)
    slot_of = jnp.sum(jnp.where(matches, earlier, 0.0), axis=1).astype(jnp.int32)
    target = (picks_flat * SLOT + slot_of).reshape(tok_count, 2)
    slot_ids = jnp.arange(slots_all, dtype=jnp.int32)[None, :]
    select_first = (target[:, 0:1] == slot_ids).astype(jnp.bfloat16)
    select_second = (target[:, 1:2] == slot_ids).astype(jnp.bfloat16)
    select_both = select_first + select_second
    outbound = jnp.einsum("ts,td->sd", select_both, normed, preferred_element_type=jnp.float32)
    outbound = outbound.astype(jnp.bfloat16).reshape(n_fs, per, SLOT, wide)

    any_spec = pl.BlockSpec(memory_space=pl.ANY)
    rows = n_gr * n_fs * blk
    bf16 = jnp.bfloat16
    dma = pltpu.SemaphoreType.DMA
    arrived, gate_new, up_new, down_new = pl.pallas_call(
        functools.partial(spread_kernel, sizes),
        out_shape=(
            jax.ShapeDtypeStruct((per, n_fs, SLOT, full_width), bf16),
            jax.ShapeDtypeStruct((per, rows, wide), bf16),
            jax.ShapeDtypeStruct((per, rows, wide), bf16),
            jax.ShapeDtypeStruct((per, rows // n_tp, full_width), bf16),
        ),
        in_specs=[any_spec] * 4,
        out_specs=(any_spec,) * 4,
        scratch_shapes=[
            pltpu.VMEM((per, SLOT, wide), bf16),
            pltpu.VMEM((3, per, blk, wide), bf16),
            dma(()),
            dma((n_fs,)),
            dma((n_tp,)),
            dma((n_tp,)),
            dma((3,)),
            dma((3, n_fs)),
            dma((3, n_gr)),
            dma((3, n_gr)),
            dma((4,)),
        ],
        compiler_params=pltpu.CompilerParams(collective_id=0, has_side_effects=True),
        name="spread",
    )(outbound, gate_cast, up_cast, down_cast)

    arrived = arrived.reshape(per, n_fs * SLOT, full_width)
    hidden, gate_new, up_new = expert_call(hidden_kernel, arrived, gate_new, up_new)
    partial_value, down_new = expert_call(down_kernel, hidden, down_new)
    partial_value = partial_value.reshape(per, n_fs, SLOT, full_width)

    vmem_spec = pl.BlockSpec(memory_space=pltpu.VMEM)
    returned = pl.pallas_call(
        functools.partial(return_kernel, sizes),
        out_shape=jax.ShapeDtypeStruct((n_fs, per, SLOT, wide), bf16),
        in_specs=[vmem_spec],
        out_specs=vmem_spec,
        scratch_shapes=[
            pltpu.VMEM((n_tp, per, n_fs, SLOT, wide), bf16),
            pltpu.VMEM((per, n_fs, SLOT, wide), bf16),
            dma((n_tp,)),
            dma((n_tp, per)),
            dma(()),
            dma((n_fs,)),
        ],
        compiler_params=pltpu.CompilerParams(collective_id=1, has_side_effects=True),
        name="give_back",
    )(partial_value)
    returned_flat = returned.reshape(slots_all, wide)
    pick_first = jnp.dot(select_first, returned_flat, preferred_element_type=jnp.float32)
    pick_second = jnp.dot(select_second, returned_flat, preferred_element_type=jnp.float32)
    mixed = route_weight[:, 0:1] * pick_first + route_weight[:, 1:2] * pick_second
    return (gate_new, up_new, down_new, mixed.astype(bf16))


def solution(mesh):
    sizes = (mesh.shape["gr"], mesh.shape["fs"], mesh.shape["tp"])
    return jax.shard_map(
        functools.partial(body, sizes),
        mesh=mesh,
        in_specs=(
            P(("gr", "fs"), "tp"),
            P(("gr", "fs")),
            P(None, ("gr", "fs"), "tp"),
            P(None, ("gr", "fs"), "tp"),
            P(None, ("gr", "fs"), "tp"),
            P(("gr", "fs"), None),
            P(("gr", "fs"), None),
        ),
        out_specs=(
            P("fs", None, "tp"),
            P("fs", None, "tp"),
            P("fs", "tp", None),
            P(("gr", "fs"), "tp"),
        ),
        check_vma=False,
    )
```

profile of v0, /device:TPU:0, one launch (start us, length us, event | category | flops | bytes accessed | tf_op | source)
XLA Modules:
  0.0 763.6 jit_solution(7998689381062198827)
XLA Ops:
  0.6 0.8 copy.17
  1.5 0.1 eq.45
  1.6 0.3 fusion.8
  1.9 0.1 convert_element_type.37
  2.1 0.1 copy.18
  2.2 0.7 multiply_add_fusion
  2.9 1.3 fusion.3
  4.2 5.9 psum.7
  10.1 0.0 copy-start.2
  10.1 3.9 convolution_convert_fusion
  14.0 0.0 slice-start
  14.0 0.0 copy-done.2
  14.0 0.0 slice-start.1
  14.0 0.0 slice-start.2
  14.0 0.0 slice-start.3
  14.0 18.2 %multiply_convert_fusion = (bf16[32,128,1024]{2,1,0:T(8,128)(2,1)}, bf16[32,128,1024]{2,1,0:T(8,128)(2,1)}) fusion(f32[32,128,1024]{2,1,0:T(8,128)} %param.10, f32[128]{0:T(128)S(1)} %copy-done.2, f32[32,128,1024]{2,1,0:T(8,128)} %param.9), kind=kLoop, calls=%fused_computation | loop fusion | flops 16777216 | bytes 50332160 | tf_op jit(solution)/shard_map/convert_element_type | solution.py:262
  32.2 0.0 slice-done
  32.2 0.9 slice-done.1
  33.1 1.3 slice-done.2
  34.4 1.2 slice-done.3
  35.6 4.0 convert_element_type.45.down
  39.6 603.3 %spread.1 = (bf16[4,8,32,2048]{3,2,1,0:T(8,128)(2,1)}, bf16[4,2048,1024]{2,1,0:T(8,128)(2,1)}, bf16[4,2048,1024]{2,1,0:T(8,128)(2,1)}, bf16[4,1024,2048]{2,1,0:T(8,128)(2,1)}) custom-call(bf16[8,4,32,1024]{3,2,1,0:T(8,128)(2,1)} %bitcast.12, bf16[32,128,1024]{2,1,0:T(8,128)(2,1)} %get-tuple-element.27.gate, bf16[32,128,1024]{2,1,0:T(8,128)(2,1)} %get-tuple-element.26.up, ...), custom_call_target="tpu_custom_call" | custom-call | tf_op jit(solution)/shard_map/spread/pallas_call | solution.py:291
  642.9 28.3 %shard_map.102 = (bf16[4,256,1024]{2,1,0:T(8,128)(2,1)}, bf16[4,2048,1024]{2,1,0:T(8,128)(2,1)}, bf16[4,2048,1024]{2,1,0:T(8,128)(2,1)}) custom-call(bf16[4,256,2048]{2,1,0:T(8,128)(2,1)} %bitcast.8, bf16[4,2048,1024]{2,1,0:T(8,128)(2,1)} %get-tuple-element.14.gate, bf16[4,2048,1024]{2,1,0:T(8,128)(2,1)} %get-tuple-element.15.up), custom_call_target="tpu_custom_call" | custom-call | tf_op jit(solution)/shard_map/pallas_call | solution.py:246
  671.2 21.7 %shard_map.103 = (bf16[4,256,2048]{2,1,0:T(8,128)(2,1)}, bf16[4,1024,2048]{2,1,0:T(8,128)(2,1)}) custom-call(bf16[4,256,1024]{2,1,0:T(8,128)(2,1)} %get-tuple-element.18.rows, bf16[4,1024,2048]{2,1,0:T(8,128)(2,1)} %get-tuple-element.19.down), custom_call_target="tpu_custom_call" | custom-call | tf_op jit(solution)/shard_map/pallas_call | solution.py:246
  693.0 0.0 copy-start.1
  693.0 66.1 %give_back.1 = bf16[8,4,32,1024]{3,2,1,0:T(8,128)(2,1)} custom-call(bf16[4,8,32,2048]{3,2,1,0:T(8,128)(2,1)} %bitcast.9), custom_call_target="tpu_custom_call" | custom-call | tf_op jit(solution)/shard_map/give_back/pallas_call | solution.py:324
  759.1 0.0 copy-done.1
  759.1 0.0 copy-start
  759.2 2.6 convolution_multiply_fusion.1
  761.8 0.0 copy-done
  761.8 1.8 fusion.2
  (6 shorter events, 0.1 us)
Async XLA Ops:
  10.1 3.9 copy-start.2
  14.0 18.2 %slice-start = ((s8[16777216]{0:T(1024)(128)(4,1)}), s8[4194304]{0:T(1024)(128)(4,1)S(1)}, s32[]{:S(2)}) async-start(s8[16777216]{0:T(1024)(128)(4,1)} %bitcast.6), calls=%async_computation | async-start | bytes 8388608
  14.0 19.1 %slice-start.1 = ((s8[16777216]{0:T(1024)(128)(4,1)}), s8[4194304]{0:T(1024)(128)(4,1)S(1)}, s32[]{:S(2)}) async-start(s8[16777216]{0:T(1024)(128)(4,1)} %bitcast.6), calls=%async_computation.1 | async-start | bytes 8388608
  14.0 20.3 %slice-start.2 = ((s8[16777216]{0:T(1024)(128)(4,1)}), s8[4194304]{0:T(1024)(128)(4,1)S(1)}, s32[]{:S(2)}) async-start(s8[16777216]{0:T(1024)(128)(4,1)} %bitcast.6), calls=%async_computation.2 | async-start | bytes 8388608
  14.0 21.5 %slice-start.3 = ((s8[16777216]{0:T(1024)(128)(4,1)}), s8[4194304]{0:T(1024)(128)(4,1)S(1)}, s32[]{:S(2)}) async-start(s8[16777216]{0:T(1024)(128)(4,1)} %bitcast.6), calls=%async_computation.3 | async-start | bytes 8388608
  693.0 66.1 %copy-start.1 = (f32[320,2]{0,1:T(2,128)S(1)}, f32[320,2]{0,1:T(2,128)}, u32[]{:S(2)}) copy-start(f32[320,2]{0,1:T(2,128)} %param.13) | copy-start | bytes 7684
  759.1 2.7 copy-start
where the time goes:
time: 764 us
  Pallas kernels  720 us (94%)
  other arithmetic  24.2 us (3%)
  matrix products  8.6 us (1%)
    pallas_call x1, Pallas kernels, body(): pl.pallas_call(functools.partial(spread_kernel, sizes), out_shape=(jax.Sh...  603 us
    pallas_call x1, Pallas kernels, body(): pl.pallas_call(functools.partial(return_kernel, sizes), out_shape=jax.Sha...  66.1 us
    pallas_call x2, Pallas kernels, expert_call(): pl.pallas_call(kernel, grid=(per, wide // tile), out_shape=(jax.ShapeDtyp...  50.1 us
    convert_element_type x1, other arithmetic, body(): up_cast = (up_weight * norm_gain[None, :, None]).astype(jnp.bfloat16)  18.2 us

commit v1 on v0

v1 whole, which is shorter than its diff:
```python
import functools

import jax
import jax.numpy as jnp
from jax import lax
from jax.experimental import pallas as pl
from jax.experimental.pallas import tpu as pltpu
from jax.sharding import PartitionSpec as P

CAP = 30
EXP_GROUP = 8
SLOT = -(-CAP // 16) * 16
GROUP_ROWS = -(-(EXP_GROUP * CAP // 2) // 128) * 128
MESH = pl.DeviceIdType.MESH
F32, BF16 = jnp.float32, jnp.bfloat16


def remote(src, dst, send, recv, device):
    copy = pltpu.make_async_remote_copy(
        src_ref=src, dst_ref=dst, send_sem=send, recv_sem=recv, device_id=device, device_id_type=MESH
    )
    copy.start()


def settle(ref, sem):
    pltpu.make_async_copy(ref, ref, sem).wait()


def loop(low, high, step):
    lax.fori_loop(low, high, lambda index, carry: (step(index), carry)[1], 0)


def span(index, size):
    return pl.ds(pl.multiple_of(index * size, size), size)


def greet(barrier, device):
    pl.semaphore_signal(barrier, inc=1, device_id=device, device_id_type=MESH)


def iota(shape, axis):
    return lax.broadcasted_iota(jnp.int32, shape, axis)


def dot(a, b):
    return jnp.dot(a, b, preferred_element_type=F32)


IN_SLOTS = 3
OUT_SLOTS = 2
EARLY = 4


def serve_kernel(
    sizes, gate, up, down, gain, prompt, routes_lane, routes_sub, weight_sub,
    gate_land, up_land, down_land, cast, mixed,
    stage_in, stage_out, prompt_pad, tok_own, meta_own, tok_land, meta_land,
    rows, pick, w_vmem, down_vmem, hidden, part, got, summed, ret,
    in_sem, out_sem, w_send, w_recv, tok_send, tok_recv, share_send, share_recv,
    meta_send, meta_recv, twin_send, twin_recv, load_sem, x_send, x_recv, z_send, z_recv,
):
    n_gr, n_fs, n_tp = sizes
    gr, fs, tp = lax.axis_index("gr"), lax.axis_index("fs"), lax.axis_index("tp")
    experts, blk, wide = gate.shape
    per = experts // n_fs
    groups = experts // EXP_GROUP
    reach = EXP_GROUP // per
    seats = n_fs // reach
    full = wide * n_tp
    toks, pad = prompt.shape[0], prompt_pad.shape[0]
    per_tp = n_gr * n_fs // n_tp
    row = gr * n_fs + fs
    owner = row // per_tp
    home = tp * per_tp // n_fs
    ring = n_fs * n_tp
    steps = per * n_fs
    weights = (gate, up, down)
    member = fs % reach
    my_group = fs // reach

    def offset(k):
        return (k + n_fs // 2 - 1) % (n_fs - 1) + 1

    def target_of(step):
        k = step % n_fs
        return jnp.where(k < n_fs - 1, (fs + offset(k)) % n_fs, fs)

    def load(step):
        e = target_of(step) * per + step // n_fs
        slot = step % IN_SLOTS
        return [
            pltpu.make_async_copy(ref.at[e], stage_in.at[slot, w], in_sem.at[slot, w])
            for w, ref in enumerate(weights)
        ]

    def start_load(step):
        for copy in load(step):
            copy.start()

    for step in range(min(IN_SLOTS, steps)):
        start_load(step)

    barrier = pltpu.get_barrier_semaphore()

    def greet_plane(k):
        other = (fs * n_tp + tp + k) % ring
        greet(barrier, (gr, other // n_tp, other % n_tp))

    loop(1, ring, greet_plane)
    loop(1, n_gr, lambda k: greet(barrier, ((gr + k) % n_gr, fs, tp)))
    pl.semaphore_wait(barrier, ring + n_gr - 2)

    def own_row(out, x, index):
        return out.at[x, span(index, blk), :]

    def down_place(x, index, t):
        return down_land.at[x, span(index, blk), span(t, wide)]

    scale = gain[...]

    def put(step):
        x, f, slot = step // n_fs, target_of(step), step % OUT_SLOTS
        e = f * per + x

        @pl.when(f != fs)
        def _():
            for w in range(3):
                pltpu.make_async_copy(stage_out.at[slot, w], cast.at[w, e], out_sem.at[slot, w]).start()

        @pl.when(f == fs)
        def _():
            for w, out in enumerate((gate_land, up_land)):
                pltpu.make_async_copy(stage_out.at[slot, w], own_row(out, x, row), out_sem.at[slot, w]).start()

            @pl.when(owner == tp)
            def _():
                place = down_place(x, row - owner * per_tp, tp)
                pltpu.make_async_copy(stage_out.at[slot, 2], place, out_sem.at[slot, 2]).start()

            @pl.when(owner != tp)
            def _():
                pltpu.make_async_copy(stage_out.at[slot, 2], cast.at[2, e], out_sem.at[slot, 2]).start()

    def dispatch(step):
        x, f, slot = step // n_fs, target_of(step), step % OUT_SLOTS
        e = f * per + x
        for w in range(3):
            settle(stage_out.at[slot, w], out_sem.at[slot, w])

        @pl.when(f != fs)
        def _():
            for w, out in enumerate((gate_land, up_land)):
                remote(cast.at[w, e], own_row(out, x, row), w_send.at[w], w_recv.at[w, x, fs], (gr, f, tp))
            place = down_place(x, row - owner * per_tp, tp)
            remote(cast.at[2, e], place, w_send.at[2], w_recv.at[2, x, fs], (gr, f, owner))

        @pl.when((f == fs) & (owner != tp))
        def _():
            place = down_place(x, row - owner * per_tp, tp)
            remote(cast.at[2, e], place, w_send.at[2], w_recv.at[2, x, fs], (gr, fs, owner))

    def cast_step(step):
        slot, out_slot = step % IN_SLOTS, step % OUT_SLOTS
        for copy in load(step):
            copy.wait()
        stage_out[out_slot, 0] = (stage_in[slot, 0] * scale).astype(BF16)
        stage_out[out_slot, 1] = (stage_in[slot, 1] * scale).astype(BF16)
        stage_out[out_slot, 2] = stage_in[slot, 2].astype(BF16)
        put(step)

        @pl.when(step > 0)
        def _():
            dispatch(step - 1)

        @pl.when(step + IN_SLOTS < steps)
        def _():
            start_load(step + IN_SLOTS)

    early = min(EARLY, steps)
    loop(0, early, cast_step)

    prompt_pad[pl.ds(0, toks), :] = prompt[...]
    if pad > toks:
        prompt_pad[pl.ds(toks, pad - toks), :] = jnp.zeros((pad - toks, wide), BF16)
    first, second = routes_lane[0:1, :], routes_lane[1:2, :]
    group_pad = -(-groups // 8) * 8
    low = iota((group_pad, pad), 0) * EXP_GROUP
    in_group = (first >= low) & (first < low + EXP_GROUP)
    expert_ids = iota((experts, pad), 0)
    named = (first == expert_ids) | (second == expert_ids)
    before = jnp.where(iota((pad, pad), 0) < iota((pad, pad), 1), 1.0, 0.0).astype(BF16)
    place_in = dot(jnp.where(in_group, 1.0, 0.0).astype(BF16), before).astype(jnp.int32)
    slot_in = dot(jnp.where(named, 1.0, 0.0).astype(BF16), before)
    slot_in = jnp.where(named, slot_in + 1.0, 0.0).astype(BF16)
    place_in = jnp.where(in_group, place_in, -1)
    for g in range(groups):
        pack = jnp.where(iota((GROUP_ROWS, pad), 0) == place_in[g : g + 1, :], 1.0, 0.0).astype(BF16)
        tok_own[g] = dot(pack, prompt_pad[...]).astype(BF16)
        meta_own[g] = lax.dot_general(
            slot_in[g * EXP_GROUP : (g + 1) * EXP_GROUP, :], pack,
            (((1,), (1,)), ((), ())), preferred_element_type=F32,
        )

    def send_tok(k):
        g = (my_group + k) % groups
        f = g * reach + member
        remote(tok_own.at[g], tok_land.at[tp, fs], tok_send, tok_recv.at[fs // reach], (gr, f, tp))

    loop(1, groups, send_tok)
    tok_land[tp, fs] = tok_own[my_group]
    meta_land[fs] = meta_own[my_group]

    def send_meta(k):
        f = (fs + k) % n_fs
        remote(meta_own.at[f // reach], meta_land.at[fs], meta_send, meta_recv, (gr, f, tp))

    loop(1, n_fs, send_meta)

    loop(early, steps, cast_step)
    dispatch(jnp.int32(steps - 1))

    def share_tok(q):
        seat = (my_group + q) % seats
        source = seat * reach + member
        place = tok_land.at[tp, source]

        @pl.when(source != fs)
        def _():
            settle(place, tok_recv.at[seat])

        def forward(j):
            seat_of = (member * n_tp + tp + j) % (reach * n_tp)
            f, t = my_group * reach + seat_of // n_tp, seat_of % n_tp
            remote(place, place, share_send, share_recv.at[tp], (gr, f, t))

        loop(1, reach * n_tp, forward)

    loop(0, seats, share_tok)

    pick_r0, pick_r1 = routes_sub[:, 0:1], routes_sub[:, 1:2]
    lane_pad = -(-experts // 128) * 128
    lanes = iota((pad, lane_pad), 1)
    named_sub = (pick_r0 == lanes) | (pick_r1 == lanes)
    before_sub = jnp.where(iota((pad, pad), 1) < iota((pad, pad), 0), 1.0, 0.0).astype(BF16)
    slots_sub = dot(before_sub, jnp.where(named_sub, 1.0, 0.0).astype(BF16))
    for j, r in enumerate((pick_r0, pick_r1)):
        slot_of = jnp.sum(jnp.where(r == lanes, slots_sub, 0.0), axis=1, keepdims=True).astype(jnp.int32)
        spot = r * SLOT + slot_of
        pick[j] = jnp.where(iota((pad, experts * SLOT), 1) == spot, 1.0, 0.0).astype(BF16)

    for j in range(n_tp):
        t = (tp + j) % n_tp
        if j > 0:
            settle(tok_land.at[t], share_recv.at[t])
        elif reach > 1:
            settle(tok_land.at[t, pl.ds(0, n_fs - seats)], share_recv.at[t])
    settle(meta_land.at[pl.ds(0, n_fs - 1)], meta_recv)

    def make_rows(source):
        total = jnp.zeros((GROUP_ROWS, 1), F32)
        for t in range(n_tp):
            values = tok_land[t, source].astype(F32)
            total = total + jnp.sum(values * values, axis=1, keepdims=True)
        factor = lax.rsqrt(total / full + 1e-06)
        for t in range(n_tp):
            normed = (tok_land[t, source].astype(F32) * factor).astype(BF16)
            for x in range(per):
                line = meta_land[source, pl.ds(member * per + x, 1), :]
                choose = jnp.where(
                    iota((SLOT, GROUP_ROWS), 0) + 1 == line.astype(jnp.int32), 1.0, 0.0
                ).astype(BF16)
                rows[x, span(source, SLOT), t * wide : (t + 1) * wide] = dot(choose, normed).astype(BF16)

    loop(0, n_fs, make_rows)

    tile = min(wide, 256)
    tile_full = min(full, 256)

    def serve(x):
        def twins(k):
            source = jnp.where(k > 0, (fs + n_fs - offset(k - 1)) % n_fs, fs)
            index = gr * n_fs + source

            @pl.when(source != fs)
            def _():
                for w, out in enumerate((gate_land, up_land)):
                    settle(own_row(out, x, index), w_recv.at[w, x, source])

            for w, out in enumerate((gate_land, up_land)):
                place = own_row(out, x, index)
                for j in range(1, n_gr):
                    g = (gr + j) % n_gr
                    remote(place, place, twin_send.at[w, g], twin_recv.at[w, x, gr], (g, fs, tp))

            @pl.when(index // per_tp == tp)
            def _():
                place = own_row(down_land, x, index - tp * per_tp)

                @pl.when(source != fs)
                def _():
                    settle(place, w_recv.at[2, x, source])

                @pl.when(source == fs)
                def _():
                    if n_tp > 1:
                        settle(down_land.at[x, span(index - tp * per_tp, blk), pl.ds(0, (n_tp - 1) * wide)], w_recv.at[2, x, fs])

                for j in range(1, n_gr):
                    g = (gr + j) % n_gr
                    remote(place, place, twin_send.at[2, g], twin_recv.at[2, x, gr], (g, fs, tp))

        loop(0, n_fs, twins)
        for j in range(1, n_gr):
            g = (gr + j) % n_gr
            for w, out in enumerate((gate_land, up_land)):
                settle(out.at[x, span(g, n_fs * blk), :], twin_recv.at[w, x, g])

        @pl.when(home != gr)
        def _():
            settle(down_land.at[x], twin_recv.at[2, x, home])

        loads = [
            pltpu.make_async_copy(gate_land.at[x], w_vmem.at[0], load_sem.at[0]),
            pltpu.make_async_copy(up_land.at[x], w_vmem.at[1], load_sem.at[1]),
            pltpu.make_async_copy(down_land.at[x], down_vmem, load_sem.at[2]),
        ]
        for copy in loads:
            copy.start()
        loads[0].wait()
        loads[1].wait()

        def hide(c):
            cut = span(c, tile)
            gate_pre = dot(rows[x], w_vmem[0, :, cut])
            up_pre = dot(rows[x], w_vmem[1, :, cut])
            hidden[:, cut] = (jax.nn.silu(gate_pre) * up_pre).astype(BF16)

        loop(0, wide // tile, hide)
        loads[2].wait()

        def lower(c):
            cut = span(c, tile_full)
            part[x, :, cut] = dot(hidden[...], down_vmem[:, cut]).astype(BF16)

        loop(0, full // tile_full, lower)
        for j in range(1, n_tp):
            t = (tp + j) % n_tp
            remote(part.at[x, :, span(t, wide)], got.at[tp, x], x_send.at[t], x_recv.at[tp, x], (gr, fs, t))
        for j in range(1, n_tp):
            t = (tp + j) % n_tp
            settle(got.at[t, x], x_recv.at[t, x])

        def add(f):
            total = part[x, span(f, SLOT), span(tp, wide)].astype(F32)
            for j in range(1, n_tp):
                total = total + got[(tp + j) % n_tp, x, span(f, SLOT), :].astype(F32)
            summed[x, span(f, SLOT), :] = total.astype(BF16)

        loop(0, n_fs, add)

        def back(k):
            f = (fs + offset(k)) % n_fs
            remote(summed.at[x, span(f, SLOT), :], ret.at[span(fs * per + x, SLOT), :], z_send, z_recv, (gr, f, tp))

        loop(0, n_fs - 1, back)
        ret[span(fs * per + x, SLOT), :] = summed[x, span(fs, SLOT), :]

    loop(0, per, serve)

    settle(ret.at[pl.ds(0, (n_fs - 1) * per * SLOT)], z_recv)

    def mix(c):
        cut = span(c, tile)
        out0 = dot(pick[0], ret[:, cut])
        out1 = dot(pick[1], ret[:, cut])
        total = weight_sub[:, 0:1] * out0 + weight_sub[:, 1:2] * out1
        mixed[:, cut] = total[0:toks].astype(BF16)

    loop(0, wide // tile, mix)

    settle(tok_own.at[pl.ds(0, groups - 1)], tok_send)
    settle(meta_land.at[pl.ds(0, n_fs - 1)], meta_send)

    def drain_share(q):
        for _ in range(reach * n_tp - 1):
            settle(tok_land.at[0, pl.ds(0, seats)], share_send)

    loop(0, 1, drain_share)
    for w in range(2):
        settle(cast.at[w, pl.ds(0, (n_fs - 1) * per)], w_send.at[w])

    @pl.when(owner == tp)
    def _():
        settle(cast.at[2, pl.ds(0, (n_fs - 1) * per)], w_send.at[2])

    @pl.when(owner != tp)
    def _():
        settle(cast.at[2], w_send.at[2])

    for j in range(1, n_gr):
        g = (gr + j) % n_gr
        for w, out in enumerate((gate_land, up_land)):
            settle(out.at[:, span(gr, n_fs * blk), :], twin_send.at[w, g])

        @pl.when(home == gr)
        def _():
            settle(down_land, twin_send.at[2, g])

    for j in range(1, n_tp):
        t = (tp + j) % n_tp
        settle(part.at[:, :, span(t, wide)], x_send.at[t])
    settle(ret.at[pl.ds(0, (n_fs - 1) * per * SLOT)], z_send)


def copy_kernel(gate, up, down, gate_out, up_out, down_out):
    gate_out[...] = gate[...]
    up_out[...] = up[...]
    down_out[...] = down[...]


def hand_over(gate, up, down):
    per = gate.shape[0]
    parts = 4

    def spec(array):
        return pl.BlockSpec((1, array.shape[1] // parts, array.shape[2]), lambda x, c: (x, c, 0))

    specs = [spec(gate), spec(up), spec(down)]
    return pl.pallas_call(
        copy_kernel,
        grid=(per, parts),
        out_shape=tuple(jax.ShapeDtypeStruct(a.shape, a.dtype) for a in (gate, up, down)),
        in_specs=specs,
        out_specs=tuple(specs),
        compiler_params=pltpu.CompilerParams(vmem_limit_bytes=60 * 1024 * 1024),
        name="hand_over",
    )(gate, up, down)


def body(sizes, prompt, norm_gain, gate_weight, up_weight, down_weight, routes, route_weight):
    n_gr, n_fs, n_tp = sizes
    tok_count, wide = prompt.shape
    full = wide * n_tp
    experts, blk, _ = gate_weight.shape
    per = experts // n_fs
    groups = experts // EXP_GROUP
    reach = EXP_GROUP // per
    seats = n_fs // reach
    rows_all = n_gr * n_fs * blk
    pad = -(-tok_count // 128) * 128
    routes_sub = jnp.pad(routes, ((0, pad - tok_count), (0, 0)), constant_values=-1)
    routes_lane = jnp.pad(routes_sub.T, ((0, 6), (0, 0)), constant_values=-1)
    weight_sub = jnp.pad(route_weight, ((0, pad - tok_count), (0, 0)))
    any_spec = pl.BlockSpec(memory_space=pl.ANY)
    vmem_spec = pl.BlockSpec(memory_space=pltpu.VMEM)
    dma = pltpu.SemaphoreType.DMA
    held = n_fs * SLOT
    gate_land, up_land, down_land, _, mixed = pl.pallas_call(
        functools.partial(serve_kernel, sizes),
        out_shape=(
            jax.ShapeDtypeStruct((per, rows_all, wide), BF16),
            jax.ShapeDtypeStruct((per, rows_all, wide), BF16),
            jax.ShapeDtypeStruct((per, rows_all // n_tp, full), BF16),
            jax.ShapeDtypeStruct((3, experts, blk, wide), BF16),
            jax.ShapeDtypeStruct((tok_count, wide), BF16),
        ),
        in_specs=[any_spec] * 3 + [vmem_spec] * 5,
        out_specs=(any_spec,) * 4 + (vmem_spec,),
        scratch_shapes=[
            pltpu.VMEM((IN_SLOTS, 3, blk, wide), F32),
            pltpu.VMEM((OUT_SLOTS, 3, blk, wide), BF16),
            pltpu.VMEM((pad, wide), BF16),
            pltpu.VMEM((groups, GROUP_ROWS, wide), BF16),
            pltpu.VMEM((groups, EXP_GROUP, GROUP_ROWS), F32),
            pltpu.VMEM((n_tp, n_fs, GROUP_ROWS, wide), BF16),
            pltpu.VMEM((n_fs, EXP_GROUP, GROUP_ROWS), F32),
            pltpu.VMEM((per, held, full), BF16),
            pltpu.VMEM((2, pad, experts * SLOT), BF16),
            pltpu.VMEM((2, rows_all, wide), BF16),
            pltpu.VMEM((rows_all // n_tp, full), BF16),
            pltpu.VMEM((held, wide), BF16),
            pltpu.VMEM((per, held, full), BF16),
            pltpu.VMEM((n_tp, per, held, wide), BF16),
            pltpu.VMEM((per, held, wide), BF16),
            pltpu.VMEM((experts * SLOT, wide), BF16),
            dma((IN_SLOTS, 3)),
            dma((OUT_SLOTS, 3)),
            dma((3,)),
            dma((3, per, n_fs)),
            dma(()),
            dma((seats,)),
            dma(()),
            dma((n_tp,)),
            dma(()),
            dma(()),
            dma((3, n_gr)),
            dma((3, per, n_gr)),
            dma((3,)),
            dma((n_tp,)),
            dma((n_tp, per)),
            dma(()),
            dma(()),
        ],
        compiler_params=pltpu.CompilerParams(
            collective_id=0, has_side_effects=True, vmem_limit_bytes=58 * 1024 * 1024
        ),
        name="serve",
    )(gate_weight, up_weight, down_weight, norm_gain.reshape(blk, 1), prompt, routes_lane, routes_sub, weight_sub)
    return (*hand_over(gate_land, up_land, down_land), mixed)


def solution(mesh):
    sizes = (mesh.shape["gr"], mesh.shape["fs"], mesh.shape["tp"])
    return jax.shard_map(
        functools.partial(body, sizes),
        mesh=mesh,
        in_specs=(
            P(("gr", "fs"), "tp"),
            P(("gr", "fs")),
            P(None, ("gr", "fs"), "tp"),
            P(None, ("gr", "fs"), "tp"),
            P(None, ("gr", "fs"), "tp"),
            P(("gr", "fs"), None),
            P(("gr", "fs"), None),
        ),
        out_specs=(
            P("fs", None, "tp"),
            P("fs", None, "tp"),
            P("fs", "tp", None),
            P(("gr", "fs"), "tp"),
        ),
        check_vma=False,
    )
```

time: 764 us -> 707 us (0.925)
  other arithmetic: 24.2 us -> 0 us
  Pallas kernels: 720 us -> 697 us
  matrix products: 8.6 us -> 0 us
    pallas_call x4 -> x2, Pallas kernels: 720 us -> 697 us  [the longest x1 661 us: body(): pl.pallas_call(functools.partial(serve_kernel, sizes), out_shape=(jax.Sha...]
    convert_element_type x3 -> x0, other arithmetic: 22.1 us -> none  [the longest x1 18.2 us: body(): up_cast = (up_weight * norm_gain[None, :, None]).astype(jnp.bfloat16)]
    dot_general x4 -> x0, matrix products: 8.6 us -> none  [the longest x1 3.89 us: body(): jnp.einsum('ts,td->sd', select_both, normed, preferred_element_type=jnp.f...]
where the time goes in v1:
time: 707 us; the launch traced here: 704 us
  Pallas kernels  697 us (99%)
    pallas_call x1, Pallas kernels, body(): pl.pallas_call(functools.partial(serve_kernel, sizes), out_shape=(jax.Sha...  661 us
    pallas_call x1, Pallas kernels, hand_over(): pl.pallas_call(copy_kernel, grid=(per, parts), out_shape=tuple((jax.Shape...  35.9 us

profile of v1, /device:TPU:0, one launch (start us, length us, event | category | flops | bytes accessed | tf_op | source)
XLA Modules:
  0.0 703.6 jit_solution(12908224063856204465)
XLA Ops:
  0.6 1.4 copy.13.gain
  2.0 0.8 copy.11
  2.8 0.8 copy.12
  3.7 0.7 pad.14.weight_sub
  4.4 0.7 fusion
  5.1 0.1 copy.15
  5.2 0.6 pad.13.clone.routes_lane
  5.8 661.0 %serve.1 = (bf16[4,2048,1024]{2,1,0:T(8,128)(2,1)}, bf16[4,2048,1024]{2,1,0:T(8,128)(2,1)}, bf16[4,1024,2048]{2,1,0:T(8,128)(2,1)}, bf16[3,32,128,1024]{3,2,1,0:T(8,128)(2,1)}, bf16[320,1024]{1,0:T(8,128)(2,1)}) custom-call(f32[32,128,1024]{2,1,0:T(8,128)} %gate.1, f32[32,128,1024]{2,1,0:T(8,128)} %up.1, f32[32,128,1024]{2,1,0:T(8,128)} %down.1, ...), custom_call_target="tpu_custom_call" | custom-call | tf_op jit(solution)/shard_map/serve/pallas_call | solution.py:458
  666.8 0.0 copy-start
  666.8 35.9 %hand_over.1 = (bf16[4,2048,1024]{2,1,0:T(8,128)(2,1)}, bf16[4,2048,1024]{2,1,0:T(8,128)(2,1)}, bf16[4,1024,2048]{2,1,0:T(8,128)(2,1)}) custom-call(bf16[4,2048,1024]{2,1,0:T(8,128)(2,1)} %get-tuple-element.11.gate, bf16[4,2048,1024]{2,1,0:T(8,128)(2,1)} %get-tuple-element.12.up, bf16[4,1024,2048]{2,1,0:T(8,128)(2,1)} %get-tuple-element.13.down), custom_call_target="tpu_custom_call" | custom-call | tf_op jit(solution)/shard_map/hand_over/pallas_call | solution.py:429
  702.7 0.0 copy-done
  702.7 0.8 copy.17
Async XLA Ops:
  666.8 35.9 %copy-start = (bf16[320,1024]{1,0:T(8,128)(2,1)S(1)}, bf16[320,1024]{1,0:T(8,128)(2,1)}, u32[]{:S(2)}) copy-start(bf16[320,1024]{1,0:T(8,128)(2,1)} %get-tuple-element.27) | copy-start | bytes 1966084

commit v2 on v1

--- a/solution.py
+++ b/solution.py
@@ -52,12 +52,12 @@
 
 
 def serve_kernel(
-    sizes, gate, up, down, gain, prompt, routes_lane, routes_sub, weight_sub,
+    sizes, gate, up, down, gain, prompt, routes, shares,
     gate_land, up_land, down_land, cast, mixed,
-    stage_in, stage_out, prompt_pad, tok_own, meta_own, tok_land, meta_land,
+    stage_in, stage_out, prompt_pad, routes_pad, shares_pad, tok_own, meta_own, tok_land, meta_land,
     rows, pick, w_vmem, down_vmem, hidden, part, got, summed, ret,
     in_sem, out_sem, w_send, w_recv, tok_send, tok_recv, share_send, share_recv,
-    meta_send, meta_recv, twin_send, twin_recv, load_sem, x_send, x_recv, z_send, z_recv,
+    meta_send, meta_recv, twin_send, twin_recv, load_sem, x_send, x_recv, z_send, z_recv, sent_sem,
 ):
     n_gr, n_fs, n_tp = sizes
     gr, fs, tp = lax.axis_index("gr"), lax.axis_index("fs"), lax.axis_index("tp")
@@ -78,15 +78,38 @@
     member = fs % reach
     my_group = fs // reach
 
-    def offset(k):
-        return (k + n_fs // 2 - 1) % (n_fs - 1) + 1
-
-    def target_of(step):
-        k = step % n_fs
-        return jnp.where(k < n_fs - 1, (fs + offset(k)) % n_fs, fs)
+    half = n_fs // 2
+    base, local = fs // half * half, fs % half
+    across = half - base
+    blocks = per * (half - 1) // 3
+    late = per * half - 2 * blocks
+    odd = per * (half - 1) - 3 * blocks
+
+    def plan(step):
+        part, rest = step % 5, step - 5 * blocks
+        early_far = step // 5 * 2 + jnp.where(part == 3, 1, 0)
+        early_near = step // 5 * 3 + jnp.where(part == 4, 2, jnp.where(part == 2, 1, 0))
+        in_early = step < 5 * blocks
+        is_far = jnp.where(in_early, (part == 0) | (part == 3), rest < late)
+        is_own = step >= 5 * blocks + late + odd
+        far = jnp.where(in_early, early_far, 2 * blocks + rest)
+        near = jnp.where(in_early, early_near, 3 * blocks + rest - late)
+        far_x, far_f = far // half, across + (local + far % half) % half
+        near_x = near // max(half - 1, 1)
+        near_f = base + (local + 1 + near % max(half - 1, 1)) % half
+        x = jnp.where(is_own, rest - late - odd, jnp.where(is_far, far_x, near_x))
+        return x, jnp.where(is_own, fs, jnp.where(is_far, far_f, near_f))
+
+    def other_to(k):
+        return jnp.where(k < half - 1, base + (local + 1 + k) % half, across + (local + k + 1 - half) % half)
+
+    def other_from(k):
+        near = base + (local + 2 * half - 1 - k) % half
+        return jnp.where(k < half - 1, near, across + (local + 2 * half - 1 - k) % half)
 
     def load(step):
-        e = target_of(step) * per + step // n_fs
+        x, f = plan(step)
+        e = f * per + x
         slot = step % IN_SLOTS
         return [
             pltpu.make_async_copy(ref.at[e], stage_in.at[slot, w], in_sem.at[slot, w])
@@ -108,18 +131,17 @@
 
     loop(1, ring, greet_plane)
     loop(1, n_gr, lambda k: greet(barrier, ((gr + k) % n_gr, fs, tp)))
-    pl.semaphore_wait(barrier, ring + n_gr - 2)
-
     def own_row(out, x, index):
         return out.at[x, span(index, blk), :]
 
     def down_place(x, index, t):
         return down_land.at[x, span(index, blk), span(t, wide)]
 
-    scale = gain[...]
+    square = iota((blk, blk), 0) == iota((blk, blk), 1)
+    scale = jnp.sum(jnp.where(square, gain[...], 0.0), axis=1, keepdims=True)
 
     def put(step):
-        x, f, slot = step // n_fs, target_of(step), step % OUT_SLOTS
+        (x, f), slot = plan(step), step % OUT_SLOTS
         e = f * per + x
 
         @pl.when(f != fs)
@@ -142,7 +164,7 @@
                 pltpu.make_async_copy(stage_out.at[slot, 2], cast.at[2, e], out_sem.at[slot, 2]).start()
 
     def dispatch(step):
-        x, f, slot = step // n_fs, target_of(step), step % OUT_SLOTS
+        (x, f), slot = plan(step), step % OUT_SLOTS
         e = f * per + x
         for w in range(3):
             settle(stage_out.at[slot, w], out_sem.at[slot, w])
@@ -159,7 +181,7 @@
             place = down_place(x, row - owner * per_tp, tp)
             remote(cast.at[2, e], place, w_send.at[2], w_recv.at[2, x, fs], (gr, fs, owner))
 
-    def cast_step(step):
+    def convert(step):
         slot, out_slot = step % IN_SLOTS, step % OUT_SLOTS
         for copy in load(step):
             copy.wait()
@@ -168,21 +190,27 @@
         stage_out[out_slot, 2] = stage_in[slot, 2].astype(BF16)
         put(step)
 
-        @pl.when(step > 0)
-        def _():
-            dispatch(step - 1)
-
         @pl.when(step + IN_SLOTS < steps)
         def _():
             start_load(step + IN_SLOTS)
 
+    def cast_step(step):
+        convert(step)
+        dispatch(step - 1)
+
     early = min(EARLY, steps)
-    loop(0, early, cast_step)
+    convert(jnp.int32(0))
+    pl.semaphore_wait(barrier, ring + n_gr - 2)
+    loop(1, early, cast_step)
 
     prompt_pad[pl.ds(0, toks), :] = prompt[...]
     if pad > toks:
         prompt_pad[pl.ds(toks, pad - toks), :] = jnp.zeros((pad - toks, wide), BF16)
-    first, second = routes_lane[0:1, :], routes_lane[1:2, :]
+    routes_pad[...] = jnp.full(routes_pad.shape, -1, jnp.int32)
+    routes_pad[0:2, 0:toks] = routes[...]
+    shares_pad[...] = jnp.zeros(shares_pad.shape, F32)
+    shares_pad[0:2, 0:toks] = shares[...]
+    first, second = routes_pad[0:1, :], routes_pad[1:2, :]
     group_pad = -(-groups // 8) * 8
     low = iota((group_pad, pad), 0) * EXP_GROUP
     in_group = (first >= low) & (first < low + EXP_GROUP)
@@ -190,8 +218,12 @@
     named = (first == expert_ids) | (second == expert_ids)
     before = jnp.where(iota((pad, pad), 0) < iota((pad, pad), 1), 1.0, 0.0).astype(BF16)
     place_in = dot(jnp.where(in_group, 1.0, 0.0).astype(BF16), before).astype(jnp.int32)
-    slot_in = dot(jnp.where(named, 1.0, 0.0).astype(BF16), before)
-    slot_in = jnp.where(named, slot_in + 1.0, 0.0).astype(BF16)
+    slot_raw = dot(jnp.where(named, 1.0, 0.0).astype(BF16), before)
+    slot_in = jnp.where(named, slot_raw + 1.0, 0.0).astype(BF16)
+    spots = []
+    for r in (first, second):
+        slot_of = jnp.sum(jnp.where(r == expert_ids, slot_raw, 0.0), axis=0, keepdims=True)
+        spots.append(r * SLOT + slot_of.astype(jnp.int32))
     place_in = jnp.where(in_group, place_in, -1)
     for g in range(groups):
         pack = jnp.where(iota((GROUP_ROWS, pad), 0) == place_in[g : g + 1, :], 1.0, 0.0).astype(BF16)
@@ -237,16 +269,14 @@
 
     loop(0, seats, share_tok)
 
-    pick_r0, pick_r1 = routes_sub[:, 0:1], routes_sub[:, 1:2]
-    lane_pad = -(-experts // 128) * 128
-    lanes = iota((pad, lane_pad), 1)
-    named_sub = (pick_r0 == lanes) | (pick_r1 == lanes)
-    before_sub = jnp.where(iota((pad, pad), 1) < iota((pad, pad), 0), 1.0, 0.0).astype(BF16)
-    slots_sub = dot(before_sub, jnp.where(named_sub, 1.0, 0.0).astype(BF16))
-    for j, r in enumerate((pick_r0, pick_r1)):
-        slot_of = jnp.sum(jnp.where(r == lanes, slots_sub, 0.0), axis=1, keepdims=True).astype(jnp.int32)
-        spot = r * SLOT + slot_of
-        pick[j] = jnp.where(iota((pad, experts * SLOT), 1) == spot, 1.0, 0.0).astype(BF16)
+    def place_picks(e):
+        ids = iota((SLOT, pad), 0) + e * SLOT
+        weight = jnp.where(ids == spots[0], shares_pad[0:1, :], 0.0) + jnp.where(ids == spots[1], shares_pad[1:2, :], 0.0)
+        high = weight.astype(BF16)
+        pick[0, span(e, SLOT), :] = high
+        pick[1, span(e, SLOT), :] = (weight - high.astype(F32)).astype(BF16)
+
+    loop(0, experts, place_picks)
 
     for j in range(n_tp):
         t = (tp + j) % n_tp
@@ -276,10 +306,36 @@
     tile = min(wide, 256)
     tile_full = min(full, 256)
 
+    def tell_sent():
+        for w in range(2):
+            settle(cast.at[w, pl.ds(0, (n_fs - 1) * per)], w_send.at[w])
+
+        @pl.when(owner == tp)
+        def _():
+            settle(cast.at[2, pl.ds(0, (n_fs - 1) * per)], w_send.at[2])
+
+        @pl.when(owner != tp)
+        def _():
+            settle(cast.at[2], w_send.at[2])
+
+        loop(1, half, lambda k: greet(sent_sem, (gr, base + (local + k) % half, tp)))
+
+    def give_back(x):
+        def back(k):
+            f = other_to(k)
+            remote(summed.at[x, span(f, SLOT), :], ret.at[span(fs * per + x, SLOT), :], z_send, z_recv, (gr, f, tp))
+
+        loop(0, n_fs - 1, back)
+        ret[span(fs * per + x, SLOT), :] = summed[x, span(fs, SLOT), :]
+
     def serve(x):
         def twins(k):
-            source = jnp.where(k > 0, (fs + n_fs - offset(k - 1)) % n_fs, fs)
+            source = jnp.where(k > 0, other_from(k - 1), fs)
             index = gr * n_fs + source
+
+            @pl.when((x == per - 1) & (k == n_fs - 1))
+            def _():
+                tell_sent()
 
             @pl.when(source != fs)
             def _():
@@ -326,6 +382,11 @@
         ]
         for copy in loads:
             copy.start()
+        @pl.when(x == per - 1)
+        def _():
+            pl.semaphore_wait(sent_sem, half - 1)
+            loop(0, per - 1, give_back)
+
         loads[0].wait()
         loads[1].wait()
 
@@ -358,12 +419,9 @@
 
         loop(0, n_fs, add)
 
-        def back(k):
-            f = (fs + offset(k)) % n_fs
-            remote(summed.at[x, span(f, SLOT), :], ret.at[span(fs * per + x, SLOT), :], z_send, z_recv, (gr, f, tp))
-
-        loop(0, n_fs - 1, back)
-        ret[span(fs * per + x, SLOT), :] = summed[x, span(fs, SLOT), :]
+        @pl.when(x == per - 1)
+        def _():
+            give_back(x)
 
     loop(0, per, serve)
 
@@ -371,9 +429,10 @@
 
     def mix(c):
         cut = span(c, tile)
-        out0 = dot(pick[0], ret[:, cut])
-        out1 = dot(pick[1], ret[:, cut])
-        total = weight_sub[:, 0:1] * out0 + weight_sub[:, 1:2] * out1
+        total = sum(
+            lax.dot_general(pick[j], ret[:, cut], (((0,), (0,)), ((), ())), preferred_element_type=F32)
+            for j in range(2)
+        )
         mixed[:, cut] = total[0:toks].astype(BF16)
 
     loop(0, wide // tile, mix)
@@ -386,17 +445,6 @@
             settle(tok_land.at[0, pl.ds(0, seats)], share_send)
 
     loop(0, 1, drain_share)
-    for w in range(2):
-        settle(cast.at[w, pl.ds(0, (n_fs - 1) * per)], w_send.at[w])
-
-    @pl.when(owner == tp)
-    def _():
-        settle(cast.at[2, pl.ds(0, (n_fs - 1) * per)], w_send.at[2])
-
-    @pl.when(owner != tp)
-    def _():
-        settle(cast.at[2], w_send.at[2])
-
     for j in range(1, n_gr):
         g = (gr + j) % n_gr
         for w, out in enumerate((gate_land, up_land)):
@@ -412,29 +460,30 @@
     settle(ret.at[pl.ds(0, (n_fs - 1) * per * SLOT)], z_send)
 
 
-def copy_kernel(gate, up, down, gate_out, up_out, down_out):
+def copy_kernel(gate, up, down, mixed, gate_out, up_out, down_out, mixed_out):
     gate_out[...] = gate[...]
     up_out[...] = up[...]
     down_out[...] = down[...]
-
-
-def hand_over(gate, up, down):
+    mixed_out[...] = mixed[...]
+
+
+def hand_over(gate, up, down, mixed):
     per = gate.shape[0]
     parts = 4
 
     def spec(array):
         return pl.BlockSpec((1, array.shape[1] // parts, array.shape[2]), lambda x, c: (x, c, 0))
 
-    specs = [spec(gate), spec(up), spec(down)]
+    specs = [spec(gate), spec(up), spec(down), pl.BlockSpec(mixed.shape, lambda x, c: (0, 0))]
     return pl.pallas_call(
         copy_kernel,
         grid=(per, parts),
-        out_shape=tuple(jax.ShapeDtypeStruct(a.shape, a.dtype) for a in (gate, up, down)),
+        out_shape=tuple(jax.ShapeDtypeStruct(a.shape, a.dtype) for a in (gate, up, down, mixed)),
         in_specs=specs,
         out_specs=tuple(specs),
         compiler_params=pltpu.CompilerParams(vmem_limit_bytes=60 * 1024 * 1024),
         name="hand_over",
-    )(gate, up, down)
+    )(gate, up, down, mixed)
 
 
 def body(sizes, prompt, norm_gain, gate_weight, up_weight, down_weight, routes, route_weight):
@@ -448,9 +497,6 @@
     seats = n_fs // reach
     rows_all = n_gr * n_fs * blk
     pad = -(-tok_count // 128) * 128
-    routes_sub = jnp.pad(routes, ((0, pad - tok_count), (0, 0)), constant_values=-1)
-    routes_lane = jnp.pad(routes_sub.T, ((0, 6), (0, 0)), constant_values=-1)
-    weight_sub = jnp.pad(route_weight, ((0, pad - tok_count), (0, 0)))
     any_spec = pl.BlockSpec(memory_space=pl.ANY)
     vmem_spec = pl.BlockSpec(memory_space=pltpu.VMEM)
     dma = pltpu.SemaphoreType.DMA
@@ -464,18 +510,20 @@
             jax.ShapeDtypeStruct((3, experts, blk, wide), BF16),
             jax.ShapeDtypeStruct((tok_count, wide), BF16),
         ),
-        in_specs=[any_spec] * 3 + [vmem_spec] * 5,
+        in_specs=[any_spec] * 3 + [vmem_spec] * 4,
         out_specs=(any_spec,) * 4 + (vmem_spec,),
         scratch_shapes=[
             pltpu.VMEM((IN_SLOTS, 3, blk, wide), F32),
             pltpu.VMEM((OUT_SLOTS, 3, blk, wide), BF16),
             pltpu.VMEM((pad, wide), BF16),
+            pltpu.VMEM((8, pad), jnp.int32),
+            pltpu.VMEM((8, pad), F32),
             pltpu.VMEM((groups, GROUP_ROWS, wide), BF16),
             pltpu.VMEM((groups, EXP_GROUP, GROUP_ROWS), F32),
             pltpu.VMEM((n_tp, n_fs, GROUP_ROWS, wide), BF16),
             pltpu.VMEM((n_fs, EXP_GROUP, GROUP_ROWS), F32),
             pltpu.VMEM((per, held, full), BF16),
-            pltpu.VMEM((2, pad, experts * SLOT), BF16),
+            pltpu.VMEM((2, experts * SLOT, pad), BF16),
             pltpu.VMEM((2, rows_all, wide), BF16),
             pltpu.VMEM((rows_all // n_tp, full), BF16),
             pltpu.VMEM((held, wide), BF16),
@@ -500,13 +548,14 @@
             dma((n_tp, per)),
             dma(()),
             dma(()),
+            pltpu.SemaphoreType.REGULAR,
         ],
         compiler_params=pltpu.CompilerParams(
             collective_id=0, has_side_effects=True, vmem_limit_bytes=58 * 1024 * 1024
         ),
         name="serve",
-    )(gate_weight, up_weight, down_weight, norm_gain.reshape(blk, 1), prompt, routes_lane, routes_sub, weight_sub)
-    return (*hand_over(gate_land, up_land, down_land), mixed)
+    )(gate_weight, up_weight, down_weight, norm_gain.reshape(1, blk), prompt, routes.T, route_weight.T)
+    return hand_over(gate_land, up_land, down_land, mixed)
 
 
 def solution(mesh):

time: 707 us -> 686 us (0.970)
  Pallas kernels: 697 us -> 679 us
    pallas_call x1, Pallas kernels: 661 us -> 642 us  [body(): pl.pallas_call(functools.partial(serve_kernel, sizes), out_shape=(jax.Sha...]
where the time goes in v2:
time: 686 us; the launch traced here: 679 us
  Pallas kernels  679 us (99%)
    pallas_call x1, Pallas kernels, body(): pl.pallas_call(functools.partial(serve_kernel, sizes), out_shape=(jax.Sha...  642 us
    pallas_call x1, Pallas kernels, hand_over(): pl.pallas_call(copy_kernel, grid=(per, parts), out_shape=tuple((jax.Shape...  36.7 us

profile of v2, /device:TPU:0, one launch (start us, length us, event | category | flops | bytes accessed | tf_op | source)
XLA Modules:
  0.0 679.4 jit_solution(6483025387906855174)
XLA Ops:
  0.6 642.1 %serve.1 = (bf16[4,2048,1024]{2,1,0:T(8,128)(2,1)}, bf16[4,2048,1024]{2,1,0:T(8,128)(2,1)}, bf16[4,1024,2048]{2,1,0:T(8,128)(2,1)}, bf16[3,32,128,1024]{3,2,1,0:T(8,128)(2,1)}, bf16[320,1024]{1,0:T(8,128)(2,1)}) custom-call(f32[32,128,1024]{2,1,0:T(8,128)} %gate.1, f32[32,128,1024]{2,1,0:T(8,128)} %up.1, f32[32,128,1024]{2,1,0:T(8,128)} %down.1, ...), custom_call_target="tpu_custom_call" | custom-call | tf_op jit(solution)/shard_map/serve/pallas_call | solution.py:504
  642.8 36.7 %hand_over.1 = (bf16[4,2048,1024]{2,1,0:T(8,128)(2,1)}, bf16[4,2048,1024]{2,1,0:T(8,128)(2,1)}, bf16[4,1024,2048]{2,1,0:T(8,128)(2,1)}, bf16[320,1024]{1,0:T(8,128)(2,1)}) custom-call(bf16[4,2048,1024]{2,1,0:T(8,128)(2,1)} %get-tuple-element.8.gate, bf16[4,2048,1024]{2,1,0:T(8,128)(2,1)} %get-tuple-element.9.up, ...), custom_call_target="tpu_custom_call" | custom-call | tf_op jit(solution)/shard_map/hand_over/pallas_call | solution.py:478

commit v3 on v2

--- a/solution.py
+++ b/solution.py
@@ -53,7 +53,7 @@
 
 def serve_kernel(
     sizes, gate, up, down, gain, prompt, routes, shares,
-    gate_land, up_land, down_land, cast, mixed,
+    pair_land, down_land, cast, mixed,
     stage_in, stage_out, prompt_pad, routes_pad, shares_pad, tok_own, meta_own, tok_land, meta_land,
     rows, pick, w_vmem, down_vmem, hidden, part, got, summed, ret,
     in_sem, out_sem, w_send, w_recv, tok_send, tok_recv, share_send, share_recv,
@@ -75,6 +75,7 @@
     ring = n_fs * n_tp
     steps = per * n_fs
     weights = (gate, up, down)
+    gate_land, up_land = pair_land.at[:, 0], pair_land.at[:, 1]
     member = fs % reach
     my_group = fs // reach
 
@@ -94,7 +95,7 @@
         is_own = step >= 5 * blocks + late + odd
         far = jnp.where(in_early, early_far, 2 * blocks + rest)
         near = jnp.where(in_early, early_near, 3 * blocks + rest - late)
-        far_x, far_f = far // half, across + (local + far % half) % half
+        far_x, far_f = far // half, across + (local + half - 1 - far % half) % half
         near_x = near // max(half - 1, 1)
         near_f = base + (local + 1 + near % max(half - 1, 1)) % half
         x = jnp.where(is_own, rest - late - odd, jnp.where(is_far, far_x, near_x))
@@ -134,6 +135,9 @@
     def own_row(out, x, index):
         return out.at[x, span(index, blk), :]
 
+    def pair_row(x, index):
+        return pair_land.at[x, :, span(index, blk), :]
+
     def down_place(x, index, t):
         return down_land.at[x, span(index, blk), span(t, wide)]
 
@@ -147,7 +151,7 @@
         @pl.when(f != fs)
         def _():
             for w in range(3):
-                pltpu.make_async_copy(stage_out.at[slot, w], cast.at[w, e], out_sem.at[slot, w]).start()
+                pltpu.make_async_copy(stage_out.at[slot, w], cast.at[e, w], out_sem.at[slot, w]).start()
 
         @pl.when(f == fs)
         def _():
@@ -161,7 +165,7 @@
 
             @pl.when(owner != tp)
             def _():
-                pltpu.make_async_copy(stage_out.at[slot, 2], cast.at[2, e], out_sem.at[slot, 2]).start()
+                pltpu.make_async_copy(stage_out.at[slot, 2], cast.at[e, 2], out_sem.at[slot, 2]).start()
 
     def dispatch(step):
         (x, f), slot = plan(step), step % OUT_SLOTS
@@ -171,15 +175,15 @@
 
         @pl.when(f != fs)
         def _():
-            for w, out in enumerate((gate_land, up_land)):
-                remote(cast.at[w, e], own_row(out, x, row), w_send.at[w], w_recv.at[w, x, fs], (gr, f, tp))
+            pair = cast.at[e, pl.ds(0, 2)]
+            remote(pair, pair_row(x, row), w_send.at[0], w_recv.at[0, x, fs], (gr, f, tp))
             place = down_place(x, row - owner * per_tp, tp)
-            remote(cast.at[2, e], place, w_send.at[2], w_recv.at[2, x, fs], (gr, f, owner))
+            remote(cast.at[e, 2], place, w_send.at[2], w_recv.at[2, x, fs], (gr, f, owner))
 
         @pl.when((f == fs) & (owner != tp))
         def _():
             place = down_place(x, row - owner * per_tp, tp)
-            remote(cast.at[2, e], place, w_send.at[2], w_recv.at[2, x, fs], (gr, fs, owner))
+            remote(cast.at[e, 2], place, w_send.at[2], w_recv.at[2, x, fs], (gr, fs, owner))
 
     def convert(step):
         slot, out_slot = step % IN_SLOTS, step % OUT_SLOTS
@@ -307,16 +311,15 @@
     tile_full = min(full, 256)
 
     def tell_sent():
-        for w in range(2):
-            settle(cast.at[w, pl.ds(0, (n_fs - 1) * per)], w_send.at[w])
+        settle(cast.at[pl.ds(0, (n_fs - 1) * per), pl.ds(0, 2)], w_send.at[0])
 
         @pl.when(owner == tp)
         def _():
-            settle(cast.at[2, pl.ds(0, (n_fs - 1) * per)], w_send.at[2])
+            settle(cast.at[pl.ds(0, (n_fs - 1) * per), 2], w_send.at[2])
 
         @pl.when(owner != tp)
         def _():
-            settle(cast.at[2], w_send.at[2])
+            settle(cast.at[:, 2], w_send.at[2])
 
         loop(1, half, lambda k: greet(sent_sem, (gr, base + (local + k) % half, tp)))
 
@@ -339,14 +342,12 @@
 
             @pl.when(source != fs)
             def _():
-                for w, out in enumerate((gate_land, up_land)):
-                    settle(own_row(out, x, index), w_recv.at[w, x, source])
-
-            for w, out in enumerate((gate_land, up_land)):
-                place = own_row(out, x, index)
-                for j in range(1, n_gr):
-                    g = (gr + j) % n_gr
-                    remote(place, place, twin_send.at[w, g], twin_recv.at[w, x, gr], (g, fs, tp))
+                settle(pair_row(x, index), w_recv.at[0, x, source])
+
+            place = pair_row(x, index)
+            for j in range(1, n_gr):
+                g = (gr + j) % n_gr
+                remote(place, place, twin_send.at[0, g], twin_recv.at[0, x, gr], (g, fs, tp))
 
             @pl.when(index // per_tp == tp)
             def _():
@@ -368,8 +369,7 @@
         loop(0, n_fs, twins)
         for j in range(1, n_gr):
             g = (gr + j) % n_gr
-            for w, out in enumerate((gate_land, up_land)):
-                settle(out.at[x, span(g, n_fs * blk), :], twin_recv.at[w, x, g])
+            settle(pair_land.at[x, :, span(g, n_fs * blk), :], twin_recv.at[0, x, g])
 
         @pl.when(home != gr)
         def _():
@@ -447,8 +447,7 @@
     loop(0, 1, drain_share)
     for j in range(1, n_gr):
         g = (gr + j) % n_gr
-        for w, out in enumerate((gate_land, up_land)):
-            settle(out.at[:, span(gr, n_fs * blk), :], twin_send.at[w, g])
+        settle(pair_land.at[:, :, span(gr, n_fs * blk), :], twin_send.at[0, g])
 
         @pl.when(home == gr)
         def _():
@@ -460,30 +459,30 @@
     settle(ret.at[pl.ds(0, (n_fs - 1) * per * SLOT)], z_send)
 
 
-def copy_kernel(gate, up, down, mixed, gate_out, up_out, down_out, mixed_out):
-    gate_out[...] = gate[...]
-    up_out[...] = up[...]
+def copy_kernel(pair, down, mixed, gate_out, up_out, down_out, mixed_out):
+    gate_out[...] = pair[:, 0]
+    up_out[...] = pair[:, 1]
     down_out[...] = down[...]
     mixed_out[...] = mixed[...]
 
 
-def hand_over(gate, up, down, mixed):
-    per = gate.shape[0]
+def hand_over(pair, down, mixed):
+    per, _, rows, wide = pair.shape
     parts = 4
-
-    def spec(array):
-        return pl.BlockSpec((1, array.shape[1] // parts, array.shape[2]), lambda x, c: (x, c, 0))
-
-    specs = [spec(gate), spec(up), spec(down), pl.BlockSpec(mixed.shape, lambda x, c: (0, 0))]
+    pair_spec = pl.BlockSpec((1, 2, rows // parts, wide), lambda x, c: (x, 0, c, 0))
+    one_spec = pl.BlockSpec((1, rows // parts, wide), lambda x, c: (x, c, 0))
+    down_spec = pl.BlockSpec((1, down.shape[1] // parts, down.shape[2]), lambda x, c: (x, c, 0))
+    mixed_spec = pl.BlockSpec(mixed.shape, lambda x, c: (0, 0))
+    one = jax.ShapeDtypeStruct((per, rows, wide), BF16)
     return pl.pallas_call(
         copy_kernel,
         grid=(per, parts),
-        out_shape=tuple(jax.ShapeDtypeStruct(a.shape, a.dtype) for a in (gate, up, down, mixed)),
-        in_specs=specs,
-        out_specs=tuple(specs),
+        out_shape=(one, one, jax.ShapeDtypeStruct(down.shape, BF16), jax.ShapeDtypeStruct(mixed.shape, BF16)),
+        in_specs=[pair_spec, down_spec, mixed_spec],
+        out_specs=(one_spec, one_spec, down_spec, mixed_spec),
         compiler_params=pltpu.CompilerParams(vmem_limit_bytes=60 * 1024 * 1024),
         name="hand_over",
-    )(gate, up, down, mixed)
+    )(pair, down, mixed)
 
 
 def body(sizes, prompt, norm_gain, gate_weight, up_weight, down_weight, routes, route_weight):
@@ -501,17 +500,16 @@
     vmem_spec = pl.BlockSpec(memory_space=pltpu.VMEM)
     dma = pltpu.SemaphoreType.DMA
     held = n_fs * SLOT
-    gate_land, up_land, down_land, _, mixed = pl.pallas_call(
+    pair_land, down_land, _, mixed = pl.pallas_call(
         functools.partial(serve_kernel, sizes),
         out_shape=(
-            jax.ShapeDtypeStruct((per, rows_all, wide), BF16),
-            jax.ShapeDtypeStruct((per, rows_all, wide), BF16),
+            jax.ShapeDtypeStruct((per, 2, rows_all, wide), BF16),
             jax.ShapeDtypeStruct((per, rows_all // n_tp, full), BF16),
-            jax.ShapeDtypeStruct((3, experts, blk, wide), BF16),
+            jax.ShapeDtypeStruct((experts, 3, blk, wide), BF16),
             jax.ShapeDtypeStruct((tok_count, wide), BF16),
         ),
         in_specs=[any_spec] * 3 + [vmem_spec] * 4,
-        out_specs=(any_spec,) * 4 + (vmem_spec,),
+        out_specs=(any_spec,) * 3 + (vmem_spec,),
         scratch_shapes=[
             pltpu.VMEM((IN_SLOTS, 3, blk, wide), F32),
             pltpu.VMEM((OUT_SLOTS, 3, blk, wide), BF16),
@@ -555,7 +553,7 @@
         ),
         name="serve",
     )(gate_weight, up_weight, down_weight, norm_gain.reshape(1, blk), prompt, routes.T, route_weight.T)
-    return hand_over(gate_land, up_land, down_land, mixed)
+    return hand_over(pair_land, down_land, mixed)
 
 
 def solution(mesh):

time: 686 us -> 682 us (level)
  no operation moved by 1% of the time
where the time goes in v3:
time: 682 us; the launch traced here: 674 us
  Pallas kernels  674 us (99%)
    pallas_call x1, Pallas kernels, body(): pl.pallas_call(functools.partial(serve_kernel, sizes), out_shape=(jax.Sha...  638 us
    pallas_call x1, Pallas kernels, hand_over(): pl.pallas_call(copy_kernel, grid=(per, parts), out_shape=(one, one, jax.S...  36.1 us

profile of v3, /device:TPU:0, one launch (start us, length us, event | category | flops | bytes accessed | tf_op | source)
XLA Modules:
  0.0 674.4 jit_solution(13280883482890384266)
XLA Ops:
  0.6 637.7 %serve.1 = (bf16[4,2,2048,1024]{3,2,1,0:T(8,128)(2,1)}, bf16[4,1024,2048]{2,1,0:T(8,128)(2,1)}, bf16[32,3,128,1024]{3,2,1,0:T(8,128)(2,1)}, bf16[320,1024]{1,0:T(8,128)(2,1)}) custom-call(f32[32,128,1024]{2,1,0:T(8,128)} %gate.1, f32[32,128,1024]{2,1,0:T(8,128)} %up.1, f32[32,128,1024]{2,1,0:T(8,128)} %down.1, f32[1,128]{1,0:T(1,128)} %bitcast.5, ...), custom_call_target="tpu_custom_call" | custom-call | tf_op jit(solution)/shard_map/serve/pallas_call | solution.py:503
  638.4 36.1 %hand_over.1 = (bf16[4,2048,1024]{2,1,0:T(8,128)(2,1)}, bf16[4,2048,1024]{2,1,0:T(8,128)(2,1)}, bf16[4,1024,2048]{2,1,0:T(8,128)(2,1)}, bf16[320,1024]{1,0:T(8,128)(2,1)}) custom-call(bf16[4,2,2048,1024]{3,2,1,0:T(8,128)(2,1)} %get-tuple-element.7.pair, bf16[4,1024,2048]{2,1,0:T(8,128)(2,1)} %get-tuple-element.8.down, bf16[320,1024]{1,0:T(8,128)(2,1)} %get-tuple-element.9.mixed), custom_call_target="tpu_custom_call" | custom-call | tf_op jit(solution)/shard_map/hand_over/pallas_call | solution.py:477
